TPU v7x, 32 devices: a whole 2x2x4 slice. The times are simulated.
32 devices in a mesh: sp: 16 (over z, y, core), tp: 2 (over x).
Axes of the slice: x: 2, y: 2, z: 4, core: 2. Of those that a mesh axis runs over, the one named last changes fastest.
Arguments:
- queries: bfloat16 [3072, 1024], P('sp', 'tp'), may hold values from -6 to 6
- keys: bfloat16 [3072, 512], P('sp', 'tp'), may hold values from -6 to 6
- values: bfloat16 [3072, 512], P('sp', 'tp'), may hold values from -6 to 6
- q_gain: float32 [64], replicated, may hold values from 0.1 to 6.5
- k_gain: float32 [64], replicated, may hold values from 0.1 to 6.5
- w_out: bfloat16 [1024, 2048], P('tp'), may hold values from -12 to 12
- residual: bfloat16 [3072, 2048], P(('sp', 'tp')), may hold values from -6 to 6
- norm_gain: float32 [2048], replicated, may hold values from 0.1 to 1.9
- w_gate: bfloat16 [2048, 5632], P('sp', 'tp'), may hold values from -0.125 to 0.125
- w_up: bfloat16 [2048, 5632], P('sp', 'tp'), may hold values from -0.125 to 0.125
- w_down: bfloat16 [5632, 2048], P('tp', 'sp'), may hold values from -0.25 to 0.25
Outputs:
- layer_out: bfloat16 [3072, 2048], P(('sp', 'tp'))
All inputs are finite; a program needn't handle non-finite values.
Results may differ from a plain program's by a relative error of at most 0.018.
The roundings to bfloat16 on the way count: a program that leaves them out, or rounds other values in their place, can miss the bound.
Values may be sent and summed in bfloat16 or wider, within the bound.
A program may use at most 128 MiB of HBM per device.

v0:
```python
import math
import jax
import jax.numpy as jnp
from jax import lax
from jax.sharding import PartitionSpec as P

GRID_W = 128
EPS = 1e-06
THETA = 10000.0


def turn_half(part, angle):
    quarter = part.shape[-1] // 2
    cos_table = jnp.cos(angle)[:, None, :]
    sin_table = jnp.sin(angle)[:, None, :]
    first_part = part[..., :quarter]
    second_part = part[..., quarter:]
    return jnp.concatenate(
        [
            first_part * cos_table - second_part * sin_table,
            first_part * sin_table + second_part * cos_table,
        ],
        axis=-1,
    )


def head_norm_rope(flat, gain, offset, head_count):
    tok_rows = flat.shape[0]
    head_size = flat.shape[1] // head_count
    heads = flat.astype(jnp.float32).reshape(tok_rows, head_count, head_size)
    heads = heads * lax.rsqrt(jnp.mean(heads * heads, axis=-1, keepdims=True) + EPS) * gain
    positions = offset + jnp.arange(tok_rows, dtype=jnp.int32)
    row_pos = (positions // GRID_W).astype(jnp.float32)
    col_pos = (positions % GRID_W).astype(jnp.float32)
    half_size = head_size // 2
    inv_freq = THETA ** (-jnp.arange(0, half_size, 2, dtype=jnp.float32) / half_size)
    turned = jnp.concatenate(
        [
            turn_half(heads[..., :half_size], row_pos[:, None] * inv_freq[None, :]),
            turn_half(heads[..., half_size:], col_pos[:, None] * inv_freq[None, :]),
        ],
        axis=-1,
    )
    return turned.reshape(tok_rows, head_count * head_size).astype(jnp.bfloat16)


def body(queries, keys, values, q_gain, k_gain, w_out, residual, norm_gain, w_gate, w_up, w_down):
    tok_rows = queries.shape[0]
    head_size = q_gain.shape[0]
    q_heads = queries.shape[1] // head_size
    kv_heads = keys.shape[1] // head_size
    q_group = q_heads // kv_heads
    offset = lax.axis_index("sp") * tok_rows
    q_rot = head_norm_rope(queries, q_gain, offset, q_heads)
    k_rot = head_norm_rope(keys, k_gain, offset, kv_heads)
    query_groups = q_rot.reshape(tok_rows, kv_heads, q_group, head_size)
    score_scale = head_size ** (-0.5)
    start_state = (
        jnp.full((kv_heads, q_group, tok_rows), -1e30, jnp.float32),
        jnp.zeros((kv_heads, q_group, tok_rows), jnp.float32),
        jnp.zeros((kv_heads, q_group, tok_rows, head_size), jnp.float32),
    )
    running = start_state
    key_piece = lax.all_gather(k_rot, "sp", axis=0, tiled=True)
    value_piece = lax.all_gather(values, "sp", axis=0, tiled=True)
    piece_len = key_piece.shape[0]
    block_len = math.gcd(piece_len, 512)
    blocks = piece_len // block_len
    key_blocks = key_piece.reshape(blocks, block_len, kv_heads, head_size)
    value_blocks = value_piece.reshape(blocks, block_len, kv_heads, head_size)

    def update(state, block_pair):
        prior_max, totals, accum = state
        key_block, value_block = block_pair
        scores = (
            jnp.einsum(
                "qhgd,khd->hgqk", query_groups, key_block, preferred_element_type=jnp.float32
            )
            * score_scale
        )
        new_max = jnp.maximum(prior_max, jnp.max(scores, axis=-1))
        weights = jnp.exp(scores - new_max[..., None])
        factor = jnp.exp(prior_max - new_max)
        totals = totals * factor + jnp.sum(weights, axis=-1)
        accum = accum * factor[..., None] + jnp.einsum(
            "hgqk,khd->hgqd",
            weights.astype(jnp.bfloat16),
            value_block,
            preferred_element_type=jnp.float32,
        )
        return ((new_max, totals, accum), None)

    running, unused = lax.scan(update, running, (key_blocks, value_blocks))
    final_max, totals, accum = running
    mixed = accum / totals[..., None]
    attn = (
        jnp.transpose(mixed, (2, 0, 1, 3))
        .reshape(tok_rows, q_heads * head_size)
        .astype(jnp.bfloat16)
    )
    own_rows = lax.all_to_all(attn, "tp", split_axis=0, concat_axis=1, tiled=True)
    columns = own_rows
    proj = jnp.dot(
        columns, lax.all_gather(w_out, "tp", axis=0, tiled=True), preferred_element_type=jnp.float32
    )
    mid = residual.astype(jnp.float32) + proj
    normed = (
        mid * lax.rsqrt(jnp.mean(mid * mid, axis=-1, keepdims=True) + EPS) * norm_gain
    ).astype(jnp.bfloat16)
    gathered = lax.all_gather(normed, "tp", axis=0, tiled=True)
    columns = gathered
    gate = jnp.dot(
        columns,
        lax.all_gather(w_gate, "sp", axis=0, tiled=True),
        preferred_element_type=jnp.float32,
    )
    up_part = jnp.dot(
        columns, lax.all_gather(w_up, "sp", axis=0, tiled=True), preferred_element_type=jnp.float32
    )
    hidden = (jax.nn.silu(gate) * up_part).astype(jnp.bfloat16)
    terms = jnp.dot(
        hidden, lax.all_gather(w_down, "sp", axis=1, tiled=True), preferred_element_type=jnp.float32
    )
    down = lax.psum_scatter(
        terms.astype(jnp.bfloat16), "tp", scatter_dimension=0, tiled=True
    ).astype(jnp.float32)
    return (mid + 0.5 * down).astype(jnp.bfloat16)


def solution(mesh):
    return jax.shard_map(
        body,
        mesh=mesh,
        in_specs=(
            P("sp", "tp"),
            P("sp", "tp"),
            P("sp", "tp"),
            P(),
            P(),
            P("tp", None),
            P(("sp", "tp"), None),
            P(),
            P("sp", "tp"),
            P("sp", "tp"),
            P("tp", "sp"),
        ),
        out_specs=P(("sp", "tp"), None),
        check_vma=False,
    )
```

profile of v0, /device:TPU:0, one launch (start us, length us, event | category | flops | bytes accessed | tf_op | source)
XLA Modules:
  0.0 477.9 jit_solution(934830852998414411)
XLA Ops:
  6.6 1.0 copy.23
  13.3 38.7 %all-gather.7.cloned.1.call-done = bf16[3072,256]{1,0:T(8,128)(2,1)} async-done(((bf16[192,256]{1,0:T(8,128)(2,1)}), bf16[3072,256]{1,0:T(8,128)(2,1)}) %all-gather.7.cloned.1.call-update) | async-done | bytes 1572880 | tf_op jit(solution)/shard_map/all_gather | solution.py:64
  52.0 4.6 reshape.207
  56.6 3.3 copy.28
  59.9 32.7 %all-gather.9.cloned.1.call-done = bf16[3072,256]{1,0:T(8,128)(2,1)} async-done(((bf16[192,256]{1,0:T(8,128)(2,1)}), bf16[3072,256]{1,0:T(8,128)(2,1)}) %all-gather.9.cloned.1.call-update) | async-done | bytes 1572880 | tf_op jit(solution)/shard_map/all_gather | solution.py:65
  92.6 4.6 reshape.208
  97.2 3.3 copy.29
  100.5 32.2 %while.15 = (s32[]{:T(128)}, f32[4,2,192]{2,1,0:T(2,128)S(1)}, f32[4,2,192]{2,1,0:T(2,128)S(1)}, f32[4,2,192,64]{2,3,1,0:T(8,128)}, bf16[6,512,4,64]{1,3,2,0:T(8...) while((s32[]{:T(128)}, f32[4,2,192]{2,1,0:T(2,128)S(1)}, ...), condition=%wide.region_5.6_spmd.clone, body=%wide.region_2.5_spmd.clone.sunk | while | flops 207920640 | bytes 14189729 | solution.py:93
  100.5 1.7 bitcast_reduce_fusion.2
  103.4 1.8 fusion.52
  106.0 1.7 bitcast_reduce_fusion.2
  108.7 1.8 fusion.52
  111.4 1.7 bitcast_reduce_fusion.2
  114.1 1.8 fusion.52
  116.7 1.7 bitcast_reduce_fusion.2
  119.4 1.8 fusion.52
  122.1 1.7 bitcast_reduce_fusion.2
  124.8 1.8 fusion.52
  127.4 1.7 bitcast_reduce_fusion.2
  130.2 1.8 fusion.52
  132.8 1.1 fusion.25
  134.2 10.3 %all_to_all.16 = bf16[2,96,512]{2,1,0:T(8,128)(2,1)S(1)} all-to-all(bf16[2,96,512]{2,1,0:T(8,128)(2,1)S(1)} %copy.30), channel_id=1, replica_groups=mesh['sp'=16,'tp'=2] {'tp'}, dimensions={0} | all-to-all | bytes 393216 | tf_op jit(solution)/shard_map/all_to_all | solution.py:101
  144.5 7.2 %all-gather.11.cloned.1.call-done = bf16[1024,2048]{1,0:T(8,128)(2,1)} async-done(((bf16[512,2048]{1,0:T(8,128)(2,1)}), bf16[1024,2048]{1,0:T(8,128)(2,1)}) %all-gather.11.cloned.1.call-update) | async-done | bytes 4194320 | tf_op jit(solution)/shard_map/all_gather | solution.py:104
  151.7 3.2 multiply_reduce_fusion
  155.1 11.5 %all_gather.24 = bf16[192,2048]{1,0:T(8,128)(2,1)S(1)} all-gather(bf16[96,2048]{1,0:T(8,128)(2,1)S(1)} %multiply_convert_fusion), channel_id=1, replica_groups=mesh['sp'=16,'tp'=2] {'tp'}, dimensions={0}, use_global_device_ids=true | all-gather | bytes 1179648 | tf_op jit(solution)/shard_map/all_gather | solution.py:110
  166.6 81.3 %all-gather.13.cloned.1.call-done = bf16[2048,2816]{1,0:T(8,128)(2,1)} async-done(((bf16[128,2816]{1,0:T(8,128)(2,1)}), bf16[2048,2816]{1,0:T(8,128)(2,1)}) %all-gather.13.cloned.1.call-update) | async-done | bytes 11534352 | tf_op jit(solution)/shard_map/all_gather | solution.py:114
  247.9 8.0 %fusion.30 = f32[192,2816]{1,0:T(8,128)} fusion(bf16[192,2048]{1,0:T(8,128)(2,1)S(1)} %all_gather.24, bf16[2048,2816]{1,0:T(8,128)(2,1)} %all-gather.13.cloned.1.call-done), kind=kOutput, calls=%fused_computation.69 | convolution fusion | flops 2214592512 | bytes 14483456 | tf_op jit(solution)/shard_map/dot_general | solution.py:112
  255.9 86.4 %all-gather.15.cloned.1.call-done = bf16[2048,2816]{1,0:T(8,128)(2,1)} async-done(((bf16[128,2816]{1,0:T(8,128)(2,1)}), bf16[2048,2816]{1,0:T(8,128)(2,1)}) %all-gather.15.cloned.1.call-update) | async-done | bytes 11534352 | tf_op jit(solution)/shard_map/all_gather | solution.py:118
  342.3 97.2 %all-gather.17.cloned.1.call-done = bf16[2816,2048]{1,0:T(8,128)(2,1)} async-done(((bf16[2816,128]{1,0:T(8,128)(2,1)}), bf16[2816,2048]{1,0:T(8,128)(2,1)}) %all-gather.17.cloned.1.call-update) | async-done | bytes 11534352 | tf_op jit(solution)/shard_map/all_gather | solution.py:122
  439.4 13.9 %convolution_convert_fusion = bf16[192,2048]{1,0:T(8,128)(2,1)} fusion(bf16[2816,2048]{1,0:T(8,128)(2,1)} %all-gather.17.cloned.1.call-done, bf16[192,2048]{1,0:T(8,128)(2,1)S(1)} %all_gather.24, bf16[2048,2816]{1,0:T(8,128)(2,1)} %all-gather.15.cloned.1.call-done, f32[192,2816]{1,0:T(8,128)} %fusion.30), kind=kOutput, calls=%fused_computation.25 | convolution fusion | flops 4432822272 | bytes 26804224 | tf_op jit(solution)/shard_map/dot_general | solution.py:121
  453.3 15.8 %reduce-scatter.2.cloned.1.call-done = bf16[96,2048]{1,0:T(8,128)(2,1)} async-done(((bf16[192,2048]{1,0:T(8,128)(2,1)}), bf16[96,2048]{1,0:T(8,128)(2,1)}) %reduce-scatter.2.cloned.1.call-update) | async-done | bytes 393232 | tf_op jit(solution)/shard_map/reduce_scatter | solution.py:124
  469.2 1.8 add_convert_fusion
  (91 shorter events, 17.0 us)
Async XLA Ops:
  6.5 6.3 %copy-start.2 = (bf16[192,512]{1,0:T(8,128)(2,1)S(1)}, bf16[192,512]{1,0:T(8,128)(2,1)}, u32[]{:S(2)}) copy-start(bf16[192,512]{1,0:T(8,128)(2,1)} %param.13) | copy-start | bytes 589828
  6.5 45.4 %all-gather.7.cloned.1.call-start = ((), (), s32[]{:S(2)}) async-start(), calls=%async_computation.2 | async-start | bytes 1671168 | tf_op jit(solution)/shard_map/all_gather | solution.py:64
  8.4 4.6 copy-start.4
  9.5 83.1 %all-gather.9.cloned.1.call-start = ((), (), s32[]{:S(2)}) async-start(), calls=%async_computation.3 | async-start | bytes 1671168 | tf_op jit(solution)/shard_map/all_gather | solution.py:65
  10.2 141.5 %all-gather.11.cloned.1.call-start = ((), (), s32[]{:S(2)}) async-start(), calls=%async_computation.4 | async-start | bytes 6291456 | tf_op jit(solution)/shard_map/all_gather | solution.py:104
  11.0 236.9 %all-gather.13.cloned.1.call-start = ((), (), s32[]{:S(2)}) async-start(), calls=%async_computation.5 | async-start | bytes 12255232 | tf_op jit(solution)/shard_map/all_gather | solution.py:114
  11.6 330.7 %all-gather.15.cloned.1.call-start = ((), (), s32[]{:S(2)}) async-start(), calls=%async_computation.6 | async-start | bytes 12255232 | tf_op jit(solution)/shard_map/all_gather | solution.py:118
  12.1 427.3 %all-gather.17.cloned.1.call-start = ((), (), s32[]{:S(2)}) async-start(), calls=%async_computation.7 | async-start | bytes 12255232 | tf_op jit(solution)/shard_map/all_gather | solution.py:122
  12.7 456.4 %reduce-scatter.2.cloned.1.call-start = ((), (), s32[]{:S(2)}) async-start(), calls=%async_computation.8 | async-start | bytes 1179648 | tf_op jit(solution)/shard_map/reduce_scatter | solution.py:124
  102.3 1.1 copy-start
  105.2 0.8 copy-start.1
  107.7 1.0 copy-start
  110.5 0.8 copy-start.1
  113.0 1.0 copy-start
  115.9 0.8 copy-start.1
  118.4 1.0 copy-start
  121.2 0.8 copy-start.1
  123.8 1.0 copy-start
  126.6 0.8 copy-start.1
  129.1 1.0 copy-start
  132.0 0.8 copy-start.1
  134.2 20.7 %copy-start.3 = (f32[2048]{0:T(1024)S(1)}, f32[2048]{0:T(1024)}, u32[]{:S(2)}) copy-start(f32[2048]{0:T(1024)} %param.20) | copy-start | bytes 24580
Sparse Core Ops, SparseCore 0:
  9.6 42.3 all-gather.6
  54.3 38.2 all-gather.8
  94.1 57.5 all-gather.10
  153.9 93.9 all-gather.12
  250.0 92.2 all-gather.14
  344.3 95.1 all-gather.16
  453.4 15.6 reduce-scatter.1
where the time goes:
time: 479 us; the launch traced here: 478 us
  waiting for transfers between devices  362 us (76%)
  matrix products  46 us (10%)
  local copies, waits for them, and re-layouts  23.4 us (5%)
  blocking collectives  21.8 us (5%)
  between operations  13.7 us (3%)
  other arithmetic  10.2 us (2%)
    all_gather x1, waiting for transfers between devices, body(): lax.all_gather(w_down, 'sp', axis=1, tiled=True)  97.2 us
    all_gather x1, waiting for transfers between devices, body(): lax.all_gather(w_up, 'sp', axis=0, tiled=True)  86.4 us
    all_gather x1, waiting for transfers between devices, body(): lax.all_gather(w_gate, 'sp', axis=0, tiled=True)  81.3 us
    all_gather x1, waiting for transfers between devices, body(): key_piece = lax.all_gather(k_rot, 'sp', axis=0, tiled=True)  38.7 us
    all_gather x1, waiting for transfers between devices, body(): value_piece = lax.all_gather(values, 'sp', axis=0, tiled=True)  32.7 us
    reduce_scatter x1, waiting for transfers between devices, body(): lax.psum_scatter(terms.astype(jnp.bfloat16), 'tp', scatter_dimension=0, t...  15.8 us
    dot_general x1, matrix products, body(): jnp.dot(hidden, lax.all_gather(w_down, 'sp', axis=1, tiled=True), preferr...  13.9 us
    all_gather x1, blocking collectives, body(): gathered = lax.all_gather(normed, 'tp', axis=0, tiled=True)  11.5 us
  transfers between devices with their start and end apart: 7, of which 7 were waited for; matrix products, arithmetic and copies ran while one was open for 12% of the time, Pallas kernels for 0%

commit v1 on v0

--- a/solution.py
+++ b/solution.py
@@ -3,6 +3,7 @@
 import jax.numpy as jnp
 from jax import lax
 from jax.sharding import PartitionSpec as P
+from jax.lax import all_gather
 
 GRID_W = 128
 EPS = 1e-06
@@ -61,8 +62,11 @@
         jnp.zeros((kv_heads, q_group, tok_rows, head_size), jnp.float32),
     )
     running = start_state
-    key_piece = lax.all_gather(k_rot, "sp", axis=0, tiled=True)
-    value_piece = lax.all_gather(values, "sp", axis=0, tiled=True)
+    key_piece, value_piece = jnp.split(
+        all_gather(jnp.concatenate([k_rot, values], axis=1), "sp", axis=0, tiled=True),
+        [k_rot.shape[1]],
+        axis=1,
+    )
     piece_len = key_piece.shape[0]
     block_len = math.gcd(piece_len, 512)
     blocks = piece_len // block_len

time: 479 us -> 443 us (0.925)
  waiting for transfers between devices: 362 us -> 325 us
  local copies, waits for them, and re-layouts: 23.4 us -> 28.2 us
    all_gather x2 -> x1, waiting for transfers between devices: 71.4 us -> 45.1 us  [body(): all_gather(jnp.concatenate([k_rot, values], axis=1), 'sp', axis=0, tiled=...]
    all_gather x1, waiting for transfers between devices: 7.22 us -> 0.02 us  [body(): lax.all_gather(w_out, 'tp', axis=0, tiled=True)]
  transfers between devices with their start and end apart: 7 -> 6, of which waited for: 7 -> 5; matrix products, arithmetic and copies ran while one was open for 12% -> 13% of each run, Pallas kernels for 0% -> 0%
where the time goes in v1:
time: 443 us; the launch traced here: 442 us
  waiting for transfers between devices  325 us (73%)
  matrix products  45.9 us (10%)
  local copies, waits for them, and re-layouts  28.2 us (6%)
  blocking collectives  18.6 us (4%)
  between operations  13.7 us (3%)
  other arithmetic  10.3 us (2%)
    all_gather x1, waiting for transfers between devices, body(): lax.all_gather(w_down, 'sp', axis=1, tiled=True)  97.2 us
    all_gather x1, waiting for transfers between devices, body(): lax.all_gather(w_up, 'sp', axis=0, tiled=True)  86.4 us
    all_gather x1, waiting for transfers between devices, body(): lax.all_gather(w_gate, 'sp', axis=0, tiled=True)  78.1 us
    all_gather x1, waiting for transfers between devices, body(): all_gather(jnp.concatenate([k_rot, values], axis=1), 'sp', axis=0, tiled=...  45.1 us
    reduce_scatter x1, waiting for transfers between devices, body(): lax.psum_scatter(terms.astype(jnp.bfloat16), 'tp', scatter_dimension=0, t...  15.8 us
    dot_general x1, matrix products, body(): jnp.dot(hidden, lax.all_gather(w_down, 'sp', axis=1, tiled=True), preferr...  13.9 us
    all_gather x1, blocking collectives, body(): gathered = lax.all_gather(normed, 'tp', axis=0, tiled=True)  11.1 us
    dot_general x6, matrix products, update(): jnp.einsum('hgqk,khd->hgqd', weights.astype(jnp.bfloat16), value_block, p...  10.8 us
  transfers between devices with their start and end apart: 6, of which 5 were waited for; matrix products, arithmetic and copies ran while one was open for 13% of the time, Pallas kernels for 0%

profile of v1, /device:TPU:0, one launch (start us, length us, event | category | flops | bytes accessed | tf_op | source)
XLA Modules:
  0.0 442.3 jit_solution(7349792426445212488)
XLA Ops:
  6.6 1.0 copy.23
  7.6 1.0 copy.24
  13.8 45.1 %all-gather.6.cloned.1.call-done = bf16[3072,512]{1,0:T(8,128)(2,1)} async-done(((bf16[192,512]{1,0:T(8,128)(2,1)}), bf16[3072,512]{1,0:T(8,128)(2,1)}) %all-gather.6.cloned.1.call-update) | async-done | bytes 3145744 | tf_op jit(solution)/shard_map/all_gather | solution.py:66
  58.9 3.7 fusion.30
  62.6 4.7 %reshape.207 = bf16[6,512,4,64]{3,2,1,0:T(4,128)(2,1)S(1)} reshape(bf16[3072,256]{1,0:T(8,128)(2,1)} %get-tuple-element.102) | data formatting | bytes 3145728 | tf_op jit(solution)/shard_map/reshape | solution.py:73
  67.3 3.3 copy.29
  70.6 4.6 %reshape.208 = bf16[6,512,4,64]{3,2,1,0:T(4,128)(2,1)S(1)} reshape(bf16[3072,256]{1,0:T(8,128)(2,1)} %get-tuple-element.101) | data formatting | bytes 3145728 | tf_op jit(solution)/shard_map/reshape | solution.py:74
  75.2 3.3 copy.30
  78.6 32.2 %while.15 = (s32[]{:T(128)}, f32[4,2,192]{2,1,0:T(2,128)S(1)}, f32[4,2,192]{2,1,0:T(2,128)S(1)}, f32[4,2,192,64]{2,3,1,0:T(8,128)}, bf16[6,512,4,64]{1,3,2,0:T(8...) while((s32[]{:T(128)}, f32[4,2,192]{2,1,0:T(2,128)S(1)}, ...), condition=%wide.region_5.6_spmd.clone, body=%wide.region_2.5_spmd.clone.sunk | while | flops 207920640 | bytes 14189729 | solution.py:97
  78.6 1.7 bitcast_reduce_fusion.2
  81.3 1.8 fusion.53
  83.9 1.7 bitcast_reduce_fusion.2
  86.7 1.8 fusion.53
  89.3 1.7 bitcast_reduce_fusion.2
  92.0 1.8 fusion.53
  94.7 1.7 bitcast_reduce_fusion.2
  97.4 1.8 fusion.53
  100.0 1.7 bitcast_reduce_fusion.2
  102.8 1.8 fusion.53
  105.4 1.7 bitcast_reduce_fusion.2
  108.1 1.8 fusion.53
  110.7 1.1 fusion.25
  112.2 7.5 %all_to_all.16 = bf16[2,96,512]{2,1,0:T(8,128)(2,1)S(1)} all-to-all(bf16[2,96,512]{2,1,0:T(8,128)(2,1)S(1)} %copy.31), channel_id=1, replica_groups=mesh['sp'=16,'tp'=2] {'tp'}, dimensions={0} | all-to-all | bytes 393216 | tf_op jit(solution)/shard_map/all_to_all | solution.py:105
  119.8 3.2 multiply_reduce_fusion
  123.1 11.1 %all_gather.20 = bf16[192,2048]{1,0:T(8,128)(2,1)S(1)} all-gather(bf16[96,2048]{1,0:T(8,128)(2,1)S(1)} %multiply_convert_fusion), channel_id=1, replica_groups=mesh['sp'=16,'tp'=2] {'tp'}, dimensions={0}, use_global_device_ids=true | all-gather | bytes 1179648 | tf_op jit(solution)/shard_map/all_gather | solution.py:114
  134.2 78.1 %all-gather.10.cloned.1.call-done = bf16[2048,2816]{1,0:T(8,128)(2,1)} async-done(((bf16[128,2816]{1,0:T(8,128)(2,1)}), bf16[2048,2816]{1,0:T(8,128)(2,1)}) %all-gather.10.cloned.1.call-update) | async-done | bytes 11534352 | tf_op jit(solution)/shard_map/all_gather | solution.py:118
  212.3 8.0 %fusion.31 = f32[192,2816]{1,0:T(8,128)} fusion(bf16[192,2048]{1,0:T(8,128)(2,1)S(1)} %all_gather.20, bf16[2048,2816]{1,0:T(8,128)(2,1)} %all-gather.10.cloned.1.call-done), kind=kOutput, calls=%fused_computation.71 | convolution fusion | flops 2214592512 | bytes 14483456 | tf_op jit(solution)/shard_map/dot_general | solution.py:116
  220.3 86.4 %all-gather.12.cloned.1.call-done = bf16[2048,2816]{1,0:T(8,128)(2,1)} async-done(((bf16[128,2816]{1,0:T(8,128)(2,1)}), bf16[2048,2816]{1,0:T(8,128)(2,1)}) %all-gather.12.cloned.1.call-update) | async-done | bytes 11534352 | tf_op jit(solution)/shard_map/all_gather | solution.py:122
  306.7 97.2 %all-gather.14.cloned.1.call-done = bf16[2816,2048]{1,0:T(8,128)(2,1)} async-done(((bf16[2816,128]{1,0:T(8,128)(2,1)}), bf16[2816,2048]{1,0:T(8,128)(2,1)}) %all-gather.14.cloned.1.call-update) | async-done | bytes 11534352 | tf_op jit(solution)/shard_map/all_gather | solution.py:126
  403.9 13.9 %convolution_convert_fusion = bf16[192,2048]{1,0:T(8,128)(2,1)} fusion(bf16[2816,2048]{1,0:T(8,128)(2,1)} %all-gather.14.cloned.1.call-done, bf16[192,2048]{1,0:T(8,128)(2,1)S(1)} %all_gather.20, bf16[2048,2816]{1,0:T(8,128)(2,1)} %all-gather.12.cloned.1.call-done, f32[192,2816]{1,0:T(8,128)} %fusion.31), kind=kOutput, calls=%fused_computation.25 | convolution fusion | flops 4432822272 | bytes 26804224 | tf_op jit(solution)/shard_map/dot_general | solution.py:125
  417.8 15.8 %reduce-scatter.2.cloned.1.call-done = bf16[96,2048]{1,0:T(8,128)(2,1)} async-done(((bf16[192,2048]{1,0:T(8,128)(2,1)}), bf16[96,2048]{1,0:T(8,128)(2,1)}) %reduce-scatter.2.cloned.1.call-update) | async-done | bytes 393232 | tf_op jit(solution)/shard_map/reduce_scatter | solution.py:128
  433.6 1.8 add_convert_fusion
  (91 shorter events, 16.6 us)
Async XLA Ops:
  6.5 52.3 %all-gather.6.cloned.1.call-start = ((), (), s32[]{:S(2)}) async-start(), calls=%async_computation.2 | async-start | bytes 3342336 | tf_op jit(solution)/shard_map/all_gather | solution.py:66
  9.4 3.9 copy-start.2
  9.7 3.9 copy-start.4
  10.6 109.2 %all-gather.8.cloned.1.call-start = ((), (), s32[]{:S(2)}) async-start(), calls=%async_computation.3 | async-start | bytes 6291456 | tf_op jit(solution)/shard_map/all_gather | solution.py:108
  11.3 201.0 %all-gather.10.cloned.1.call-start = ((), (), s32[]{:S(2)}) async-start(), calls=%async_computation.4 | async-start | bytes 12255232 | tf_op jit(solution)/shard_map/all_gather | solution.py:118
  12.0 294.7 %all-gather.12.cloned.1.call-start = ((), (), s32[]{:S(2)}) async-start(), calls=%async_computation.5 | async-start | bytes 12255232 | tf_op jit(solution)/shard_map/all_gather | solution.py:122
  12.6 391.3 %all-gather.14.cloned.1.call-start = ((), (), s32[]{:S(2)}) async-start(), calls=%async_computation.6 | async-start | bytes 12255232 | tf_op jit(solution)/shard_map/all_gather | solution.py:126
  13.2 420.4 %reduce-scatter.2.cloned.1.call-start = ((), (), s32[]{:S(2)}) async-start(), calls=%async_computation.7 | async-start | bytes 1179648 | tf_op jit(solution)/shard_map/reduce_scatter | solution.py:128
  80.3 1.0 copy-start
  83.1 0.8 copy-start.1
  85.6 1.0 copy-start
  88.5 0.8 copy-start.1
  91.0 1.0 copy-start
  93.8 0.8 copy-start.1
  96.3 1.0 copy-start
  99.2 0.8 copy-start.1
  101.7 1.0 copy-start
  104.6 0.8 copy-start.1
  107.1 1.0 copy-start
  109.9 0.8 copy-start.1
  112.2 10.8 %copy-start.3 = (f32[2048]{0:T(1024)S(1)}, f32[2048]{0:T(1024)}, u32[]{:S(2)}) copy-start(f32[2048]{0:T(1024)} %param.20) | copy-start | bytes 24580
Sparse Core Ops, SparseCore 0:
  10.7 48.1 all-gather.5
  60.4 55.0 all-gather.7
  117.8 94.4 all-gather.9
  214.5 92.2 all-gather.11
  308.7 95.1 all-gather.13
  417.9 15.6 reduce-scatter.1
